TPU v7x, 512 devices: a whole 4x4x16 slice. The times are simulated.
512 devices in a mesh: sp: 32 (over z, core), tp: 16 (over y, x).
Axes of the slice: x: 4, y: 4, z: 16, core: 2. Of those that a mesh axis runs over, the one named last changes fastest.
Arguments:
- u_val: bfloat16 [8192, 2048], P('sp', 'tp'), may hold values from -6 to 6
- u_gate: bfloat16 [8192, 2048], P('sp', 'tp'), may hold values from -9 to 9
- conv_weight: float32 [31, 2048], P(None, 'tp')
- conv_bias: float32 [2048], P('tp'), may hold values from -3 to 3
- ln_gain: float32 [2048], P('tp'), may hold values from 0.1 to 1.9
- ln_bias: float32 [2048], P('tp'), may hold values from -3 to 3
- proj_weight: bfloat16 [2048, 4096], P(None, 'tp'), may hold values from -0.125 to 0.125
- resid: bfloat16 [8192, 4096], P('sp', 'tp')
- norm_gain: float32 [4096], P('tp'), may hold values from 0.1 to 1.9
- route_ids: int32 [8192, 2], P('sp'), may hold values from 0 to 31, all different within a row; in each aligned block of 256 rows (0 to 255, 256 to 511, ...) at most 32 rows name the same one
- route_wts: float32 [8192, 2], P('sp'), may hold values from 0.3 to 1.5
- expert_gate: bfloat16 [32, 4096, 1024], P('sp', None, 'tp'), may hold values from -0.09375 to 0.09375
- expert_up: bfloat16 [32, 4096, 1024], P('sp', None, 'tp'), may hold values from -0.09375 to 0.09375
- expert_down: bfloat16 [32, 1024, 4096], P('sp', None, 'tp'), may hold values from -0.1875 to 0.1875
- shared_gate: bfloat16 [4096, 1024], P(None, 'tp'), may hold values from -0.09375 to 0.09375
- shared_up: bfloat16 [4096, 1024], P(None, 'tp'), may hold values from -0.09375 to 0.09375
- shared_down: bfloat16 [1024, 4096], P(None, 'tp'), may hold values from -0.1875 to 0.1875
Outputs:
- mixed: bfloat16 [8192, 4096], P('sp', 'tp')
Inputs may be any that keep to these rules, and one draw needn't show every extreme that they name: `route_ids`: each row names 2 different experts. In each aligned block of 256 rows (the rows of one index of sp) no expert is named by more than 32 rows, a bound that some expert reaches in some blocks.
All inputs are finite; a program needn't handle non-finite values.
Results may differ from a plain program's by a relative error of at most 0.012.
Values may be sent and summed in bfloat16 or wider, within the bound.
A program may use at most 64 MiB of HBM per device.

v0:
```python
import jax
import jax.numpy as jnp
from jax import lax
from jax.sharding import PartitionSpec as P

D = 4096
CONV = 2048
norm_eps = 1e-06


def shifted(block, axis, distance):
    devices = range(lax.axis_size(axis))
    route = [(i - distance, i) for i in devices if i - distance in devices]
    return lax.ppermute(block, axis, route)


def from_everyone(array, axis):
    size = lax.axis_size(axis)
    return lax.all_to_all(
        jnp.broadcast_to(array[None], (size, *array.shape)), axis, 0, 0, tiled=True
    )


def over_copies(array, axis):
    return from_everyone(array, axis).sum(axis=0)


def in_one(arrays, axis):
    ravelled, at, gathered = (jnp.concatenate([a.reshape(-1) for a in arrays]), 0, [])
    subtotal = over_copies(ravelled, axis)
    for a in arrays:
        gathered.append(subtotal[at : at + a.size].reshape(a.shape))
        at += a.size
    return tuple(gathered)


def laid_out(pieces, dim):
    dims = list(pieces.shape[1:])
    dims[dim] *= pieces.shape[0]
    return jnp.moveaxis(pieces, 0, dim).reshape(dims)


def gather_directly(array, axis, dim):
    return laid_out(from_everyone(array, axis), dim)


def rows_first(arrays, axis, dims):
    turned = [jnp.moveaxis(a, dim, 0) for a, dim in zip(arrays, dims)]
    widths = [t[0].size for t in turned]
    both = jnp.concatenate([t.reshape(-1, w) for t, w in zip(turned, widths)], axis=1)
    out = lax.all_gather(both, axis, axis=0, tiled=True)
    pieces = jnp.split(out, [sum(widths[:k]) for k in range(1, len(widths))], axis=1)
    return tuple(
        (
            jnp.moveaxis(b.reshape(-1, *t.shape[1:]), 0, dim)
            for b, t, dim in zip(pieces, turned, dims)
        )
    )


def shards(
    u_val,
    u_gate,
    conv_weight,
    conv_bias,
    ln_gain,
    ln_bias,
    proj_weight,
    resid,
    norm_gain,
    route_ids,
    route_wts,
    expert_gate,
    expert_up,
    expert_down,
    shared_gate,
    shared_up,
    shared_down,
):
    tok_rows = u_val.shape[0]
    sp_count = lax.axis_size("sp")
    tp_count = lax.axis_size("tp")
    kernel_width = conv_weight.shape[0]
    gated = (u_val.astype(jnp.float32) * jax.nn.sigmoid(u_gate.astype(jnp.float32))).astype(
        jnp.bfloat16
    )
    rim_rows = shifted(gated[tok_rows - (kernel_width - 1) :], "sp", 1)
    padded = lax.optimization_barrier(jnp.concatenate([rim_rows, gated], axis=0)).astype(
        jnp.float32
    )
    conv_sum = jnp.zeros((tok_rows, gated.shape[1]), jnp.float32) + conv_bias[None, :]
    for tap_index in range(kernel_width):
        conv_sum = (
            conv_sum + conv_weight[tap_index][None, :] * padded[tap_index : tap_index + tok_rows]
        )
    stat_sums = in_one((jnp.sum(conv_sum, axis=1), jnp.sum(conv_sum * conv_sum, axis=1)), "tp")
    channel_mean = stat_sums[0] / CONV
    channel_var = stat_sums[1] / CONV - channel_mean * channel_mean
    normed_conv = (conv_sum - channel_mean[:, None]) * lax.rsqrt(channel_var + norm_eps)[:, None]
    conv_out = jax.nn.silu(normed_conv * ln_gain + ln_bias).astype(jnp.bfloat16)
    projected = jnp.dot(
        gather_directly(conv_out, "tp", 1), proj_weight, preferred_element_type=jnp.float32
    )
    residual_mid = (resid.astype(jnp.float32) + projected).astype(jnp.bfloat16)
    residual_wide = residual_mid.astype(jnp.float32)
    square_sum = over_copies(jnp.sum(residual_wide * residual_wide, axis=1), "tp")
    normed_rows = (
        residual_wide * lax.rsqrt(square_sum / D + norm_eps)[:, None] * norm_gain
    ).astype(jnp.bfloat16)
    rows_full = gather_directly(normed_rows, "tp", 1)
    topk_count = route_ids.shape[1]
    capacity = 2 * tok_rows * topk_count // sp_count
    pair_ids = route_ids.reshape(-1)
    onehot = (pair_ids[:, None] == jnp.arange(sp_count, dtype=jnp.int32)[None, :]).astype(jnp.int32)
    before = jnp.cumsum(onehot, axis=0) - onehot
    position = jnp.sum(before * onehot, axis=1)
    pair_slot = pair_ids * capacity + position
    matches = (
        jnp.arange(sp_count * capacity, dtype=jnp.int32)[:, None] == pair_slot[None, :]
    ).astype(jnp.int32)
    pair_tok = jnp.arange(tok_rows * topk_count, dtype=jnp.int32) // topk_count
    filled = jnp.sum(matches, axis=1)
    slot_tok = jnp.sum(matches * pair_tok[None, :], axis=1) + (1 - filled) * tok_rows
    rows_ext = jnp.concatenate(
        [rows_full, jnp.zeros((1, rows_full.shape[1]), jnp.bfloat16)], axis=0
    )
    part_slots = capacity // tp_count
    tp_index = lax.axis_index("tp")
    local_slots = lax.dynamic_slice_in_dim(
        slot_tok.reshape(sp_count, capacity), tp_index * part_slots, part_slots, 1
    )
    send_rows = jnp.take(rows_ext, local_slots.reshape(-1), axis=0).reshape(
        sp_count, part_slots, -1
    )
    received = lax.all_to_all(send_rows, "sp", split_axis=0, concat_axis=0, tiled=True)
    arrived = lax.all_gather(received, "tp", axis=1, tiled=True)
    slot_rows = arrived.reshape(sp_count * capacity, -1)
    gate_pre = jnp.dot(slot_rows, expert_gate[0], preferred_element_type=jnp.float32)
    up_proj = jnp.dot(slot_rows, expert_up[0], preferred_element_type=jnp.float32)
    hidden = (jax.nn.silu(gate_pre) * up_proj).astype(jnp.bfloat16)
    shared_pre = jnp.dot(rows_full, shared_gate, preferred_element_type=jnp.float32)
    shared_upper = jnp.dot(rows_full, shared_up, preferred_element_type=jnp.float32)
    shared_hidden = (jax.nn.silu(shared_pre) * shared_upper).astype(jnp.bfloat16)
    out_cols = expert_down.shape[2]
    pieces = rows_first((hidden, shared_hidden), "tp", (1, 1))
    routed_rows = expert_down[0]
    routed_out = jnp.dot(pieces[0], routed_rows, preferred_element_type=jnp.float32)
    shared_out = jnp.dot(pieces[1], shared_down, preferred_element_type=jnp.float32)
    expert_rows = routed_out.astype(jnp.bfloat16).reshape(sp_count, capacity, out_cols)
    returned_rows = lax.all_to_all(expert_rows, "sp", split_axis=0, concat_axis=0, tiled=True)
    returned_flat = returned_rows.reshape(sp_count * capacity, out_cols)
    picked = (
        jnp.take(returned_flat, pair_slot, axis=0)
        .astype(jnp.float32)
        .reshape(tok_rows, topk_count, out_cols)
    )
    routed = jnp.sum(picked * route_wts[:, :, None], axis=1)
    return (residual_wide + shared_out + routed).astype(jnp.bfloat16)


def solution(mesh):
    in_specs = (
        P("sp", "tp"),
        P("sp", "tp"),
        P(None, "tp"),
        P("tp"),
        P("tp"),
        P("tp"),
        P(None, "tp"),
        P("sp", "tp"),
        P("tp"),
        P("sp", None),
        P("sp", None),
        P("sp", None, "tp"),
        P("sp", None, "tp"),
        P("sp", None, "tp"),
        P(None, "tp"),
        P(None, "tp"),
        P(None, "tp"),
    )
    out_specs = P("sp", "tp")
    return jax.shard_map(shards, mesh=mesh, in_specs=in_specs, out_specs=out_specs, check_vma=False)
```

profile of v0, /device:TPU:1, one launch (start us, length us, event | category | flops | bytes accessed | tf_op | source)
XLA Modules:
  0.0 380.0 jit_solution(2414357554840305814)
XLA Ops:
  6.5 1.0 multiply_convert_fusion.2
  7.6 4.9 %collective-permute-start = (bf16[30,128]{1,0:T(8,128)(2,1)S(1)}, bf16[30,128]{1,0:T(8,128)(2,1)S(1)}, u32[]{:S(2)}, u32[]{:S(2)}) collective-permute-start(bf16[30,128]{1,0:T(8,128)(2,1)S(1)} %slice.272), channel_id=1, source_target_pairs={{0,16},{16,32},{32,48},{48,64},{64,80},{80,96},{96,112},{112,128},... | collective-permute-start | bytes 23048 | tf_op jit(solution)/shard_map/ppermute | solution.py:14
  12.5 1.0 slice_bitcast_fusion.30
  13.5 1.0 slice_bitcast_fusion.29
  14.5 1.9 collective-permute-done
  16.4 1.3 fusion.56
  17.7 11.3 %all_to_all.32 = f32[16,1,512]{2,1,0:T(1,128)S(1)} all-to-all(f32[16,1,512]{2,1,0:T(1,128)S(1)} %broadcast_in_dim.22), channel_id=1, replica_groups=mesh['sp'=32,'tp'=16] {'tp'}, dimensions={0} | all-to-all | bytes 65536 | tf_op jit(solution)/shard_map/all_to_all | solution.py:19
  29.1 0.2 multiply_convert_fusion.1
  29.4 1.1 broadcast_in_dim.23
  30.5 3.8 all-to-all-start.1
  34.4 16.9 %all-to-all-done.1 = bf16[16,256,128]{1,2,0:T(8,128)(2,1)S(1)} async-done(((bf16[16,256,128]{1,2,0:T(8,128)(2,1)}), bf16[16,256,128]{1,2,0:T(8,128)(2,1)S(1)}, u32[]{:S(2)}, u32[]{:S(2)}) %all-to-all-start.1) | async-done | bytes 1048608 | tf_op jit(solution)/shard_map/all_to_all | solution.py:19
  51.3 0.5 multiply_reduce_fusion.1
  51.9 10.3 %all_to_all.33 = f32[16,1,256]{2,1,0:T(1,128)S(1)} all-to-all(f32[16,1,256]{2,1,0:T(1,128)S(1)} %broadcast_in_dim.25), channel_id=1, replica_groups=mesh['sp'=32,'tp'=16] {'tp'}, dimensions={0} | all-to-all | bytes 32768 | tf_op jit(solution)/shard_map/all_to_all | solution.py:19
  62.4 1.6 broadcast_in_dim.26
  64.0 3.8 %all-to-all-start.3 = ((bf16[16,256,256]{2,1,0:T(8,128)(2,1)}), bf16[16,256,256]{2,1,0:T(8,128)(2,1)S(1)}, u32[]{:S(2)}, u32[]{:S(2)}) async-start(bf16[16,256,256]{2,1,0:T(8,128)(2,1)} %broadcast_in_dim.26), calls=%async_computation.3 | async-start | bytes 4194304 | tf_op jit(solution)/shard_map/all_to_all | solution.py:19
  68.0 0.1 reshape.176
  68.2 0.1 eq.40
  68.3 1.2 reduce-window.6
  69.5 0.2 slice_reduce_fusion
  69.9 0.6 convert_reduce_fusion
  70.8 24.7 %all-to-all-done.3 = bf16[16,256,256]{2,1,0:T(8,128)(2,1)S(1)} async-done(((bf16[16,256,256]{2,1,0:T(8,128)(2,1)}), bf16[16,256,256]{2,1,0:T(8,128)(2,1)S(1)}, u32[]{:S(2)}, u32[]{:S(2)}) %all-to-all-start.3) | async-done | bytes 2097184 | tf_op jit(solution)/shard_map/all_to_all | solution.py:19
  95.5 1.3 copy-done.2
  96.8 1.8 copy.131
  98.7 1.6 concatenate.14
  100.2 4.1 %gather_fusion = bf16[64,4096]{1,0:T(8,128)(2,1)} fusion(bf16[257,4096]{1,0:T(8,128)(2,1)} %concatenate.14, s32[1024]{0:T(1024)S(1)} %pad_clamp_fusion.1), kind=kCustom, calls=%fused_computation | custom fusion | bytes 1048832 | tf_op jit(solution)/shard_map/jit(_take)/gather | solution.py:132
  104.3 2.2 gather.13
  106.4 1.6 broadcast_select_fusion
  108.1 52.7 %all_to_all.34 = bf16[32,2,4096]{2,1,0:T(2,128)(2,1)S(1)} all-to-all(bf16[32,2,4096]{2,1,0:T(2,128)(2,1)S(1)} %broadcast_select_fusion), channel_id=1, replica_groups=mesh['sp'=32,'tp'=16] {'sp'}, dimensions={0} | all-to-all | bytes 1048576 | tf_op jit(solution)/shard_map/all_to_all | solution.py:135
  160.8 1.1 copy.116
  162.0 0.2 all-gather.5.cloned.1.call-start
  162.2 1.9 convolution_bitcast_fusion.3
  164.1 0.8 fusion.12
  164.8 70.4 %all-gather.3.cloned.1.call-done = bf16[32,32,4096]{2,0,1:T(8,128)(2,1)} async-done(((bf16[32,2,4096]{2,0,1:T(8,128)(2,1)}), bf16[32,32,4096]{2,0,1:T(8,128)(2,1)}) %all-gather.3.cloned.1.call-update) | async-done | bytes 8388624 | tf_op jit(solution)/shard_map/all_gather | solution.py:136
  235.3 11.2 %copy.117 = bf16[32,32,4096]{2,1,0:T(8,128)(2,1)} copy(bf16[32,32,4096]{2,0,1:T(8,128)(2,1)} %all-gather.3.cloned.1.call-done) | data formatting | bytes 16777216 | tf_op jit(solution)/shard_map/all_gather | solution.py:136
  246.5 6.2 %convolution_bitcast_fusion.1 = f32[64,1024]{1,0:T(8,128)S(1)} fusion(bf16[1024,4096]{1,0:T(8,128)(2,1)} %bitcast.128, bf16[1,4096,64]{1,2,0:T(8,128)(2,1)S(1)} %copy-done.3), kind=kOutput, calls=%fused_computation.9 | convolution fusion | flops 536870912 | bytes 9175040 | tf_op jit(solution)/shard_map/dot_general | solution.py:138
  252.7 2.7 fusion.9
  255.3 0.7 pad_maximum_fusion
  256.1 60.2 %all-gather.5.cloned.1.call-done = bf16[1024,1280]{1,0:T(8,128)(2,1)} async-done(((bf16[64,1280]{1,0:T(8,128)(2,1)}), bf16[1024,1280]{1,0:T(8,128)(2,1)}) %all-gather.5.cloned.1.call-update) | async-done | bytes 2621456 | tf_op jit(solution)/shard_map/all_gather | solution.py:51
  316.3 3.2 fusion.2
  319.5 14.3 %all-to-all-start.5 = ((bf16[32,32,256]{2,1,0:T(8,128)(2,1)}), bf16[32,32,256]{2,1,0:T(8,128)(2,1)S(1)}, u32[]{:S(2)}, u32[]{:S(2)}) async-start(bf16[32,32,256]{2,1,0:T(8,128)(2,1)} %bitcast.44), calls=%async_computation.5 | async-start | bytes 1048576 | tf_op jit(solution)/shard_map/all_to_all | solution.py:150
  333.8 0.1 reduce_sum.93
  334.1 0.1 mul.553
  334.3 0.2 copy.120
  334.7 32.6 %all-to-all-done.5 = bf16[32,32,256]{2,1,0:T(8,128)(2,1)S(1)} async-done(((bf16[32,32,256]{2,1,0:T(8,128)(2,1)}), bf16[32,32,256]{2,1,0:T(8,128)(2,1)S(1)}, u32[]{:S(2)}, u32[]{:S(2)}) %all-to-all-start.5) | async-done | bytes 524320 | tf_op jit(solution)/shard_map/all_to_all | solution.py:150
  367.3 1.9 gather_fusion.1
  369.4 1.5 multiply_reduce_fusion
  371.0 1.4 fusion.10
  372.4 0.8 copy.124
  (65 shorter events, 1.9 us)
Async XLA Ops:
  6.5 44.8 %copy-start = (bf16[2048,256]{1,0:T(8,128)(2,1)S(1)}, bf16[2048,256]{1,0:T(8,128)(2,1)}, u32[]{:S(2)}) copy-start(bf16[2048,256]{1,0:T(8,128)(2,1)} %param.23) | copy-start | bytes 3145732
  7.6 8.8 %collective-permute-start = (bf16[30,128]{1,0:T(8,128)(2,1)S(1)}, bf16[30,128]{1,0:T(8,128)(2,1)S(1)}, u32[]{:S(2)}, u32[]{:S(2)}) collective-permute-start(bf16[30,128]{1,0:T(8,128)(2,1)S(1)} %slice.272), channel_id=1, source_target_pairs={{0,16},{16,32},{32,48},{48,64},{64,80},{80,96},{96,112},{112,128},... | collective-permute-start | bytes 23048 | tf_op jit(solution)/shard_map/ppermute | solution.py:14
  16.4 12.7 %copy-start.10 = (f32[128]{0:T(128)S(1)}, f32[128]{0:T(128)}, u32[]{:S(2)}) copy-start(f32[128]{0:T(128)} %param.22) | copy-start | bytes 1540
  16.4 12.7 %copy-start.11 = (f32[128]{0:T(128)S(1)}, f32[128]{0:T(128)}, u32[]{:S(2)}) copy-start(f32[128]{0:T(128)} %param.21) | copy-start | bytes 1540
  17.7 16.6 %copy-start.6 = (bf16[256,256]{1,0:T(8,128)(2,1)S(1)}, bf16[256,256]{1,0:T(8,128)(2,1)}, u32[]{:S(2)}) copy-start(bf16[256,256]{1,0:T(8,128)(2,1)} %param.24) | copy-start | bytes 393220
  30.5 31.7 %copy-start.9 = (f32[256]{0:T(256)S(1)}, f32[256]{0:T(256)}, u32[]{:S(2)}) copy-start(f32[256]{0:T(256)} %param.25) | copy-start | bytes 3076
  30.5 20.8 %all-to-all-start.1 = ((bf16[16,256,128]{1,2,0:T(8,128)(2,1)}), bf16[16,256,128]{1,2,0:T(8,128)(2,1)S(1)}, u32[]{:S(2)}, u32[]{:S(2)}) async-start(bf16[16,256,128]{1,2,0:T(8,128)(2,1)} %broadcast_in_dim.23), calls=%async_computation.1 | async-start | bytes 2097152 | tf_op jit(solution)/shard_map/all_to_all | solution.py:19
  64.0 3.9 %copy-start.7 = (s32[256,2]{0,1:T(2,128)S(1)}, s32[256,2]{0,1:T(2,128)}, u32[]{:S(2)}) copy-start(s32[256,2]{0,1:T(2,128)} %param.26) | copy-start | bytes 6148
  64.0 31.5 %all-to-all-start.3 = ((bf16[16,256,256]{2,1,0:T(8,128)(2,1)}), bf16[16,256,256]{2,1,0:T(8,128)(2,1)S(1)}, u32[]{:S(2)}, u32[]{:S(2)}) async-start(bf16[16,256,256]{2,1,0:T(8,128)(2,1)} %broadcast_in_dim.26), calls=%async_computation.3 | async-start | bytes 4194304 | tf_op jit(solution)/shard_map/all_to_all | solution.py:19
  67.8 167.5 %all-gather.3.cloned.1.call-start = ((), (), s32[]{:S(2)}) async-start(), calls=%async_computation.6 | async-start | bytes 8912896 | tf_op jit(solution)/shard_map/all_gather | solution.py:136
  95.5 1.4 copy-start.2
  162.0 154.3 %all-gather.5.cloned.1.call-start = ((), (), s32[]{:S(2)}) async-start(), calls=%async_computation.7 | async-start | bytes 2785280 | tf_op jit(solution)/shard_map/all_gather | solution.py:51
  162.2 1.9 copy-start.5
  164.8 81.6 %copy-start.3 = (bf16[1,4096,64]{1,2,0:T(8,128)(2,1)S(1)}, bf16[1,4096,64]{1,2,0:T(8,128)(2,1)}, u32[]{:S(2)}) copy-start(bf16[1,4096,64]{1,2,0:T(8,128)(2,1)} %param.28) | copy-start | bytes 1572868
  246.5 6.2 %copy-start.1 = (bf16[32,32,4096]{2,1,0:T(8,128)(2,1)S(1)}, bf16[32,32,4096]{2,1,0:T(8,128)(2,1)}, u32[]{:S(2)}) copy-start(bf16[32,32,4096]{2,1,0:T(8,128)(2,1)} %copy.117) | copy-start | bytes 25165828
  246.5 6.2 %copy-start.12 = (bf16[1,4096,64]{1,2,0:T(8,128)(2,1)S(1)}, bf16[1,4096,64]{1,2,0:T(8,128)(2,1)}, u32[]{:S(2)}) copy-start(bf16[1,4096,64]{1,2,0:T(8,128)(2,1)} %param.29) | copy-start | bytes 1572868
  252.7 63.6 %copy-start.13 = (bf16[1,1024,256]{2,1,0:T(8,128)(2,1)S(1)}, bf16[1,1024,256]{2,1,0:T(8,128)(2,1)}, u32[]{:S(2)}) copy-start(bf16[1,1024,256]{2,1,0:T(8,128)(2,1)} %param.30) | copy-start | bytes 1572868
  256.0 78.5 %copy-start.8 = (f32[256,2]{0,1:T(2,128)S(1)}, f32[256,2]{0,1:T(2,128)}, u32[]{:S(2)}) copy-start(f32[256,2]{0,1:T(2,128)} %param.27) | copy-start | bytes 6148
  319.5 47.8 %all-to-all-start.5 = ((bf16[32,32,256]{2,1,0:T(8,128)(2,1)}), bf16[32,32,256]{2,1,0:T(8,128)(2,1)S(1)}, u32[]{:S(2)}, u32[]{:S(2)}) async-start(bf16[32,32,256]{2,1,0:T(8,128)(2,1)} %bitcast.44), calls=%async_computation.5 | async-start | bytes 1048576 | tf_op jit(solution)/shard_map/all_to_all | solution.py:150
  334.5 36.5 %copy-start.4 = (bf16[1024,256]{1,0:T(8,128)(2,1)S(1)}, bf16[1024,256]{1,0:T(8,128)(2,1)}, u32[]{:S(2)}) copy-start(bf16[1024,256]{1,0:T(8,128)(2,1)} %param.33) | copy-start | bytes 1572868
Sparse Core Ops, SparseCore 0:
  162.1 73.1 all-gather.2
  256.2 60.0 all-gather.4
where the time goes:
time: 381 us; the launch traced here: 380 us
  waiting for transfers between devices  207 us (54%)
  blocking collectives  74.3 us (20%)
  local copies, waits for them, and re-layouts  32.9 us (9%)
  starting transfers between devices  27.1 us (7%)
  matrix products  16.6 us (4%)
  between operations  13.8 us (4%)
  other arithmetic  8.53 us (2%)
    all_gather x1, waiting for transfers between devices, shards(): arrived = lax.all_gather(received, 'tp', axis=1, tiled=True)  70.4 us
    all_gather x1, waiting for transfers between devices, rows_first(): out = lax.all_gather(both, axis, axis=0, tiled=True)  60.2 us
    all_to_all x1, blocking collectives, shards(): lax.all_to_all(send_rows, 'sp', split_axis=0, concat_axis=0, tiled=True)  52.7 us
    all_to_all x2, waiting for transfers between devices, from_everyone(): lax.all_to_all(jnp.broadcast_to(array[None], (size, *array.shape)), axis,...  41.6 us
    all_to_all x1, waiting for transfers between devices, shards(): lax.all_to_all(expert_rows, 'sp', split_axis=0, concat_axis=0, tiled=True)  32.6 us
    all_to_all x2, blocking collectives, from_everyone(): lax.all_to_all(jnp.broadcast_to(array[None], (size, *array.shape)), axis,...  21.6 us
    all_to_all x1, starting transfers between devices, shards(): lax.all_to_all(expert_rows, 'sp', split_axis=0, concat_axis=0, tiled=True)  14.3 us
    all_gather x1, local copies, waits for them, and re-layouts, shards(): arrived = lax.all_gather(received, 'tp', axis=1, tiled=True)  11.2 us
  transfers between devices with their start and end apart: 6, of which 6 were waited for; matrix products, arithmetic and copies ran while one was open for 2% of the time, Pallas kernels for 0%

commit v1 on v0

--- a/solution.py
+++ b/solution.py
@@ -6,6 +6,27 @@
 D = 4096
 CONV = 2048
 norm_eps = 1e-06
+
+
+def collect(x, axis, dim):
+    size, position, width = (lax.axis_size(axis), lax.axis_index(axis), x.shape[dim])
+    ahead = [(i, (i + 1) % size) for i in range(size)]
+    downward = [(i, (i - 1) % size) for i in range(size)]
+    out = jnp.zeros((*x.shape[:dim], size * width, *x.shape[dim + 1 :]), x.dtype)
+    out = lax.dynamic_update_slice_in_dim(out, x, position * width, axis=dim)
+    from_left = from_right = x
+    halfway = size // 2
+    for step in range(1, halfway + 1):
+        from_left = lax.ppermute(from_left, axis, ahead)
+        out = lax.dynamic_update_slice_in_dim(
+            out, from_left, (position - step) % size * width, axis=dim
+        )
+        if step < size - halfway:
+            from_right = lax.ppermute(from_right, axis, downward)
+            out = lax.dynamic_update_slice_in_dim(
+                out, from_right, (position + step) % size * width, axis=dim
+            )
+    return out
 
 
 def shifted(block, axis, distance):
@@ -133,7 +154,7 @@
         sp_count, part_slots, -1
     )
     received = lax.all_to_all(send_rows, "sp", split_axis=0, concat_axis=0, tiled=True)
-    arrived = lax.all_gather(received, "tp", axis=1, tiled=True)
+    arrived = collect(received, "tp", 1)
     slot_rows = arrived.reshape(sp_count * capacity, -1)
     gate_pre = jnp.dot(slot_rows, expert_gate[0], preferred_element_type=jnp.float32)
     up_proj = jnp.dot(slot_rows, expert_up[0], preferred_element_type=jnp.float32)

time: 381 us -> 416 us (1.092)
  starting transfers between devices: 27.1 us -> 109 us
  blocking collectives: 74.3 us -> 21.4 us
    all_gather x1 -> x0, waiting for transfers between devices: 70.4 us -> none  [shards(): arrived = lax.all_gather(received, 'tp', axis=1, tiled=True)]
    ppermute x0 -> x15, starting transfers between devices: none -> 62.4 us  [the longest x7 47 us: collect(): from_right = lax.ppermute(from_right, axis, downward)]
    all_to_all x1 -> x0, blocking collectives: 52.7 us -> none  [shards(): lax.all_to_all(send_rows, 'sp', split_axis=0, concat_axis=0, tiled=True)]
    ppermute x0 -> x15, waiting for transfers between devices: none -> 44.4 us  [the longest x8 44.4 us: collect(): from_left = lax.ppermute(from_left, axis, ahead)]
    all_to_all x0 -> x1, waiting for transfers between devices: none -> 31.4 us  [shards(): lax.all_to_all(send_rows, 'sp', split_axis=0, concat_axis=0, tiled=True)]
    all_to_all x0 -> x1, starting transfers between devices: none -> 19.5 us  [shards(): lax.all_to_all(send_rows, 'sp', split_axis=0, concat_axis=0, tiled=True)]
    dynamic_update_slice x0 -> x16, local copies, waits for them, and re-layouts: none -> 13.7 us  [the longest x8 6.3 us: collect(): lax.dynamic_update_slice_in_dim(out, from_left, (position - step) % size...]
    all_gather x1 -> x0, local copies, waits for them, and re-layouts: 11.2 us -> none  [shards(): arrived = lax.all_gather(received, 'tp', axis=1, tiled=True)]
  transfers between devices with their start and end apart: 6 -> 21, of which waited for: 6 -> 14; matrix products, arithmetic and copies ran while one was open for 2% -> 6% of each run, Pallas kernels for 0% -> 0%
where the time goes in v1:
time: 416 us; the launch traced here: 415 us
  waiting for transfers between devices  211 us (51%)
  starting transfers between devices  109 us (26%)
  local copies, waits for them, and re-layouts  35.3 us (8%)
  blocking collectives  21.4 us (5%)
  between operations  14.4 us (3%)
  matrix products  14 us (3%)
  other arithmetic  9.99 us (2%)
    all_gather x1, waiting for transfers between devices, rows_first(): out = lax.all_gather(both, axis, axis=0, tiled=True)  59.3 us
    ppermute x7, starting transfers between devices, collect(): from_right = lax.ppermute(from_right, axis, downward)  47 us
    ppermute x8, waiting for transfers between devices, collect(): from_left = lax.ppermute(from_left, axis, ahead)  44.4 us
    all_to_all x2, waiting for transfers between devices, from_everyone(): lax.all_to_all(jnp.broadcast_to(array[None], (size, *array.shape)), axis,...  41.6 us
    all_to_all x1, waiting for transfers between devices, shards(): lax.all_to_all(expert_rows, 'sp', split_axis=0, concat_axis=0, tiled=True)  32.6 us
    all_to_all x1, waiting for transfers between devices, shards(): lax.all_to_all(send_rows, 'sp', split_axis=0, concat_axis=0, tiled=True)  31.4 us
    all_to_all x2, blocking collectives, from_everyone(): lax.all_to_all(jnp.broadcast_to(array[None], (size, *array.shape)), axis,...  21.4 us
    all_to_all x1, starting transfers between devices, shards(): lax.all_to_all(send_rows, 'sp', split_axis=0, concat_axis=0, tiled=True)  19.5 us
  transfers between devices with their start and end apart: 21, of which 14 were waited for; matrix products, arithmetic and copies ran while one was open for 6% of the time, Pallas kernels for 0%

profile of v1, /device:TPU:1, one launch (start us, length us, event | category | flops | bytes accessed | tf_op | source)
XLA Modules:
  0.0 414.9 jit_solution(12258645355059588128)
XLA Ops:
  7.6 4.9 %collective-permute-start = (bf16[30,128]{1,0:T(8,128)(2,1)S(1)}, bf16[30,128]{1,0:T(8,128)(2,1)S(1)}, u32[]{:S(2)}, u32[]{:S(2)}) collective-permute-start(bf16[30,128]{1,0:T(8,128)(2,1)S(1)} %slice.272), channel_id=1, source_target_pairs={{0,16},{16,32},{32,48},{48,64},{64,80},{80,96},{96,112},{112,128},... | collective-permute-start | bytes 23048 | tf_op jit(solution)/shard_map/ppermute | solution.py:35
  14.5 1.9 collective-permute-done
  17.7 11.1 %all_to_all.32 = f32[16,1,512]{2,1,0:T(1,128)S(1)} all-to-all(f32[16,1,512]{2,1,0:T(1,128)S(1)} %broadcast_in_dim.24), channel_id=1, replica_groups=mesh['sp'=32,'tp'=16] {'tp'}, dimensions={0} | all-to-all | bytes 65536 | tf_op jit(solution)/shard_map/all_to_all | solution.py:40
  30.9 3.7 all-to-all-start.1
  34.7 16.9 %all-to-all-done.1 = bf16[16,256,128]{1,2,0:T(8,128)(2,1)S(1)} async-done(((bf16[16,256,128]{1,2,0:T(8,128)(2,1)}), bf16[16,256,128]{1,2,0:T(8,128)(2,1)S(1)}, u32[]{:S(2)}, u32[]{:S(2)}) %all-to-all-start.1) | async-done | bytes 1048608 | tf_op jit(solution)/shard_map/all_to_all | solution.py:40
  52.2 10.3 %all_to_all.33 = f32[16,1,256]{2,1,0:T(1,128)S(1)} all-to-all(f32[16,1,256]{2,1,0:T(1,128)S(1)} %broadcast_in_dim.28), channel_id=1, replica_groups=mesh['sp'=32,'tp'=16] {'tp'}, dimensions={0} | all-to-all | bytes 32768 | tf_op jit(solution)/shard_map/all_to_all | solution.py:40
  64.3 3.7 all-to-all-start.3
  71.0 24.7 %all-to-all-done.3 = bf16[16,256,256]{2,1,0:T(8,128)(2,1)S(1)} async-done(((bf16[16,256,256]{2,1,0:T(8,128)(2,1)}), bf16[16,256,256]{2,1,0:T(8,128)(2,1)S(1)}, u32[]{:S(2)}, u32[]{:S(2)}) %all-to-all-start.3) | async-done | bytes 2097184 | tf_op jit(solution)/shard_map/all_to_all | solution.py:40
  97.0 1.8 copy.94
  98.9 1.6 concatenate.14
  100.5 4.1 gather_fusion
  104.5 2.2 gather.13
  106.7 2.4 broadcast_select_fusion
  109.1 19.5 %all-to-all-start.4 = ((bf16[32,2,4096]{2,1,0:T(2,128)(2,1)}), bf16[32,2,4096]{2,1,0:T(2,128)(2,1)}, u32[]{:S(2)}, u32[]{:S(2)}) async-start(bf16[32,2,4096]{2,1,0:T(2,128)(2,1)} %broadcast_select_fusion), calls=%async_computation.4 | async-start | bytes 1048576 | tf_op jit(solution)/shard_map/all_to_all | solution.py:156
  128.9 1.8 convolution_bitcast_fusion.3
  130.7 31.4 %all-to-all-done.4 = bf16[32,2,4096]{2,1,0:T(2,128)(2,1)} async-done(((bf16[32,2,4096]{2,1,0:T(2,128)(2,1)}), bf16[32,2,4096]{2,1,0:T(2,128)(2,1)}, u32[]{:S(2)}, u32[]{:S(2)}) %all-to-all-start.4) | async-done | bytes 524320 | tf_op jit(solution)/shard_map/all_to_all | solution.py:156
  162.1 1.9 collective-permute-start.1
  164.1 6.7 %collective-permute-start.2 = (bf16[32,2,4096]{2,1,0:T(2,128)(2,1)}, bf16[32,2,4096]{2,1,0:T(2,128)(2,1)S(1)}, u32[]{:S(2)}, u32[]{:S(2)}) collective-permute-start(bf16[32,2,4096]{2,1,0:T(2,128)(2,1)} %all-to-all-done.4), channel_id=1, source_target_pairs={{0,15},{1,0},{2,1},{3,2},{4,3},{5,4},{6,5},{7,6},{8,7},{9,8},{10,9... | collective-permute-start | bytes 1572872 | tf_op jit(solution)/shard_map/ppermute | solution.py:25
  170.7 1.8 fusion.10
  173.6 1.9 constant_dynamic-update-slice_fusion.15
  175.5 5.0 %collective-permute-done.1 = bf16[32,2,4096]{2,1,0:T(2,128)(2,1)S(1)} collective-permute-done((bf16[32,2,4096]{2,1,0:T(2,128)(2,1)}, bf16[32,2,4096]{2,1,0:T(2,128)(2,1)S(1)}, u32[]{:S(2)}, u32[]{:S(2)}) %collective-permute-start.1) | collective-permute-done | bytes 524320 | tf_op jit(solution)/shard_map/ppermute | solution.py:20
  180.5 1.9 collective-permute-start.3
  182.5 6.9 %collective-permute-start.4 = (bf16[32,2,4096]{2,1,0:T(2,128)(2,1)S(1)}, bf16[32,2,4096]{2,1,0:T(2,128)(2,1)S(1)}, u32[]{:S(2)}, u32[]{:S(2)}) collective-permute-start(bf16[32,2,4096]{2,1,0:T(2,128)(2,1)S(1)} %collective-permute-done.2), channel_id=1, source_target_pairs={{0,15},{1,0},{2,1},{3,2},{4,3},{5,4},{6,5},{7,6},{8,7},{9,8},{10,9... | collective-permute-start | bytes 1572872 | tf_op jit(solution)/shard_map/ppermute | solution.py:25
  190.9 6.9 %collective-permute-done.3 = bf16[32,2,4096]{2,1,0:T(2,128)(2,1)S(1)} collective-permute-done((bf16[32,2,4096]{2,1,0:T(2,128)(2,1)S(1)}, bf16[32,2,4096]{2,1,0:T(2,128)(2,1)S(1)}, u32[]{:S(2)}, u32[]{:S(2)}) %collective-permute-start.3) | collective-permute-done | bytes 524320 | tf_op jit(solution)/shard_map/ppermute | solution.py:20
  197.9 1.9 collective-permute-start.5
  199.8 6.7 %collective-permute-start.6 = (bf16[32,2,4096]{2,1,0:T(2,128)(2,1)S(1)}, bf16[32,2,4096]{2,1,0:T(2,128)(2,1)S(1)}, u32[]{:S(2)}, u32[]{:S(2)}) collective-permute-start(bf16[32,2,4096]{2,1,0:T(2,128)(2,1)S(1)} %collective-permute-done.4), channel_id=1, source_target_pairs={{0,15},{1,0},{2,1},{3,2},{4,3},{5,4},{6,5},{7,6},{8,7},{9,8},{10,9... | collective-permute-start | bytes 1572872 | tf_op jit(solution)/shard_map/ppermute | solution.py:25
  208.1 6.3 %collective-permute-done.5 = bf16[32,2,4096]{2,1,0:T(2,128)(2,1)S(1)} collective-permute-done((bf16[32,2,4096]{2,1,0:T(2,128)(2,1)S(1)}, bf16[32,2,4096]{2,1,0:T(2,128)(2,1)S(1)}, u32[]{:S(2)}, u32[]{:S(2)}) %collective-permute-start.5) | collective-permute-done | bytes 524320 | tf_op jit(solution)/shard_map/ppermute | solution.py:20
  214.3 1.9 collective-permute-start.7
  216.3 6.7 %collective-permute-start.8 = (bf16[32,2,4096]{2,1,0:T(2,128)(2,1)S(1)}, bf16[32,2,4096]{2,1,0:T(2,128)(2,1)S(1)}, u32[]{:S(2)}, u32[]{:S(2)}) collective-permute-start(bf16[32,2,4096]{2,1,0:T(2,128)(2,1)S(1)} %collective-permute-done.6), channel_id=1, source_target_pairs={{0,15},{1,0},{2,1},{3,2},{4,3},{5,4},{6,5},{7,6},{8,7},{9,8},{10,9... | collective-permute-start | bytes 1572872 | tf_op jit(solution)/shard_map/ppermute | solution.py:25
  224.5 5.4 %collective-permute-done.7 = bf16[32,2,4096]{2,1,0:T(2,128)(2,1)S(1)} collective-permute-done((bf16[32,2,4096]{2,1,0:T(2,128)(2,1)S(1)}, bf16[32,2,4096]{2,1,0:T(2,128)(2,1)S(1)}, u32[]{:S(2)}, u32[]{:S(2)}) %collective-permute-start.7) | collective-permute-done | bytes 524320 | tf_op jit(solution)/shard_map/ppermute | solution.py:20
  229.9 1.9 collective-permute-start.9
  231.9 6.7 %collective-permute-start.10 = (bf16[32,2,4096]{2,1,0:T(2,128)(2,1)S(1)}, bf16[32,2,4096]{2,1,0:T(2,128)(2,1)S(1)}, u32[]{:S(2)}, u32[]{:S(2)}) collective-permute-start(bf16[32,2,4096]{2,1,0:T(2,128)(2,1)S(1)} %collective-permute-done.8), channel_id=1, source_target_pairs={{0,15},{1,0},{2,1},{3,2},{4,3},{5,4},{6,5},{7,6},{8,7},{9,8},{10,9... | collective-permute-start | bytes 1572872 | tf_op jit(solution)/shard_map/ppermute | solution.py:25
  240.2 4.5 %collective-permute-done.9 = bf16[32,2,4096]{2,1,0:T(2,128)(2,1)S(1)} collective-permute-done((bf16[32,2,4096]{2,1,0:T(2,128)(2,1)S(1)}, bf16[32,2,4096]{2,1,0:T(2,128)(2,1)S(1)}, u32[]{:S(2)}, u32[]{:S(2)}) %collective-permute-start.9) | collective-permute-done | bytes 524320 | tf_op jit(solution)/shard_map/ppermute | solution.py:20
  244.7 1.9 collective-permute-start.11
  246.6 6.7 %collective-permute-start.12 = (bf16[32,2,4096]{2,1,0:T(2,128)(2,1)S(1)}, bf16[32,2,4096]{2,1,0:T(2,128)(2,1)S(1)}, u32[]{:S(2)}, u32[]{:S(2)}) collective-permute-start(bf16[32,2,4096]{2,1,0:T(2,128)(2,1)S(1)} %collective-permute-done.10), channel_id=1, source_target_pairs={{0,15},{1,0},{2,1},{3,2},{4,3},{5,4},{6,5},{7,6},{8,7},{9,8},{10,9... | collective-permute-start | bytes 1572872 | tf_op jit(solution)/shard_map/ppermute | solution.py:25
  254.9 3.7 collective-permute-done.11
  258.6 1.9 collective-permute-start.13
  260.5 6.7 %collective-permute-start.14 = (bf16[32,2,4096]{2,1,0:T(2,128)(2,1)S(1)}, bf16[32,2,4096]{2,1,0:T(2,128)(2,1)S(1)}, u32[]{:S(2)}, u32[]{:S(2)}) collective-permute-start(bf16[32,2,4096]{2,1,0:T(2,128)(2,1)S(1)} %collective-permute-done.12), channel_id=1, source_target_pairs={{0,15},{1,0},{2,1},{3,2},{4,3},{5,4},{6,5},{7,6},{8,7},{9,8},{10,9... | collective-permute-start | bytes 1572872 | tf_op jit(solution)/shard_map/ppermute | solution.py:25
  268.8 3.0 collective-permute-done.13
  271.8 2.1 collective-permute-start.15
  275.6 9.5 %collective-permute-done.15 = bf16[32,2,4096]{2,1,0:T(2,128)(2,1)S(1)} collective-permute-done((bf16[32,2,4096]{2,1,0:T(2,128)(2,1)S(1)}, bf16[32,2,4096]{2,1,0:T(2,128)(2,1)S(1)}, u32[]{:S(2)}, u32[]{:S(2)}) %collective-permute-start.15) | collective-permute-done | bytes 524320 | tf_op jit(solution)/shard_map/ppermute | solution.py:20
  285.9 2.7 convolution_bitcast_fusion.1
  288.6 2.7 multiply_convert_fusion
  292.0 59.3 %all-gather.2.cloned.1.call-done = bf16[1024,1280]{1,0:T(8,128)(2,1)} async-done(((bf16[64,1280]{1,0:T(8,128)(2,1)}), bf16[1024,1280]{1,0:T(8,128)(2,1)}) %all-gather.2.cloned.1.call-update) | async-done | bytes 2621456 | tf_op jit(solution)/shard_map/all_gather | solution.py:72
  351.2 3.2 fusion.2
  354.4 14.3 %all-to-all-start.5 = ((bf16[32,32,256]{2,1,0:T(8,128)(2,1)}), bf16[32,32,256]{2,1,0:T(8,128)(2,1)S(1)}, u32[]{:S(2)}, u32[]{:S(2)}) async-start(bf16[32,32,256]{2,1,0:T(8,128)(2,1)} %bitcast.44), calls=%async_computation.5 | async-start | bytes 1048576 | tf_op jit(solution)/shard_map/all_to_all | solution.py:171
  369.6 32.6 %all-to-all-done.5 = bf16[32,32,256]{2,1,0:T(8,128)(2,1)S(1)} async-done(((bf16[32,32,256]{2,1,0:T(8,128)(2,1)}), bf16[32,32,256]{2,1,0:T(8,128)(2,1)S(1)}, u32[]{:S(2)}, u32[]{:S(2)}) %all-to-all-start.5) | async-done | bytes 524320 | tf_op jit(solution)/shard_map/all_to_all | solution.py:171
  402.2 1.9 gather_fusion.1
  (100 shorter events, 31.4 us)
Async XLA Ops:
  6.5 45.1 %copy-start = (bf16[2048,256]{1,0:T(8,128)(2,1)S(1)}, bf16[2048,256]{1,0:T(8,128)(2,1)}, u32[]{:S(2)}) copy-start(bf16[2048,256]{1,0:T(8,128)(2,1)} %param.23) | copy-start | bytes 3145732
  6.5 28.1 %copy-start.4 = (bf16[256,256]{1,0:T(8,128)(2,1)S(1)}, bf16[256,256]{1,0:T(8,128)(2,1)}, u32[]{:S(2)}) copy-start(bf16[256,256]{1,0:T(8,128)(2,1)} %param.24) | copy-start | bytes 393220
  6.5 56.0 %copy-start.7 = (f32[256]{0:T(256)S(1)}, f32[256]{0:T(256)}, u32[]{:S(2)}) copy-start(f32[256]{0:T(256)} %param.25) | copy-start | bytes 3076
  7.6 8.8 %collective-permute-start = (bf16[30,128]{1,0:T(8,128)(2,1)S(1)}, bf16[30,128]{1,0:T(8,128)(2,1)S(1)}, u32[]{:S(2)}, u32[]{:S(2)}) collective-permute-start(bf16[30,128]{1,0:T(8,128)(2,1)S(1)} %slice.272), channel_id=1, source_target_pairs={{0,16},{16,32},{32,48},{48,64},{64,80},{80,96},{96,112},{112,128},... | collective-permute-start | bytes 23048 | tf_op jit(solution)/shard_map/ppermute | solution.py:35
  16.4 51.6 %copy-start.5 = (s32[256,2]{0,1:T(2,128)S(1)}, s32[256,2]{0,1:T(2,128)}, u32[]{:S(2)}) copy-start(s32[256,2]{0,1:T(2,128)} %param.26) | copy-start | bytes 6148
  30.9 20.7 %all-to-all-start.1 = ((bf16[16,256,128]{1,2,0:T(8,128)(2,1)}), bf16[16,256,128]{1,2,0:T(8,128)(2,1)S(1)}, u32[]{:S(2)}, u32[]{:S(2)}) async-start(bf16[16,256,128]{1,2,0:T(8,128)(2,1)} %broadcast_in_dim.25), calls=%async_computation.1 | async-start | bytes 2097152 | tf_op jit(solution)/shard_map/all_to_all | solution.py:40
  64.3 31.4 %all-to-all-start.3 = ((bf16[16,256,256]{2,1,0:T(8,128)(2,1)}), bf16[16,256,256]{2,1,0:T(8,128)(2,1)S(1)}, u32[]{:S(2)}, u32[]{:S(2)}) async-start(bf16[16,256,256]{2,1,0:T(8,128)(2,1)} %broadcast_in_dim.29), calls=%async_computation.3 | async-start | bytes 4194304 | tf_op jit(solution)/shard_map/all_to_all | solution.py:40
  95.7 1.3 copy-start.1
  109.1 53.1 %all-to-all-start.4 = ((bf16[32,2,4096]{2,1,0:T(2,128)(2,1)}), bf16[32,2,4096]{2,1,0:T(2,128)(2,1)}, u32[]{:S(2)}, u32[]{:S(2)}) async-start(bf16[32,2,4096]{2,1,0:T(2,128)(2,1)} %broadcast_select_fusion), calls=%async_computation.4 | async-start | bytes 1048576 | tf_op jit(solution)/shard_map/all_to_all | solution.py:156
  128.6 222.7 %all-gather.2.cloned.1.call-start = ((), (), s32[]{:S(2)}) async-start(), calls=%async_computation.6 | async-start | bytes 2785280 | tf_op jit(solution)/shard_map/all_gather | solution.py:72
  162.1 18.4 %collective-permute-start.1 = (bf16[32,2,4096]{2,1,0:T(2,128)(2,1)}, bf16[32,2,4096]{2,1,0:T(2,128)(2,1)S(1)}, u32[]{:S(2)}, u32[]{:S(2)}) collective-permute-start(bf16[32,2,4096]{2,1,0:T(2,128)(2,1)} %all-to-all-done.4), channel_id=1, source_target_pairs={{0,1},{1,2},{2,3},{3,4},{4,5},{5,6},{6,7},{7,8},{8,9},{9,10},{10,1... | collective-permute-start | bytes 1572872 | tf_op jit(solution)/shard_map/ppermute | solution.py:20
  164.1 18.4 %collective-permute-start.2 = (bf16[32,2,4096]{2,1,0:T(2,128)(2,1)}, bf16[32,2,4096]{2,1,0:T(2,128)(2,1)S(1)}, u32[]{:S(2)}, u32[]{:S(2)}) collective-permute-start(bf16[32,2,4096]{2,1,0:T(2,128)(2,1)} %all-to-all-done.4), channel_id=1, source_target_pairs={{0,15},{1,0},{2,1},{3,2},{4,3},{5,4},{6,5},{7,6},{8,7},{9,8},{10,9... | collective-permute-start | bytes 1572872 | tf_op jit(solution)/shard_map/ppermute | solution.py:25
  173.6 112.3 %copy-start.2 = (bf16[1,4096,64]{1,2,0:T(8,128)(2,1)S(1)}, bf16[1,4096,64]{1,2,0:T(8,128)(2,1)}, u32[]{:S(2)}) copy-start(bf16[1,4096,64]{1,2,0:T(8,128)(2,1)} %param.28) | copy-start | bytes 1572868
  180.5 17.3 %collective-permute-start.3 = (bf16[32,2,4096]{2,1,0:T(2,128)(2,1)S(1)}, bf16[32,2,4096]{2,1,0:T(2,128)(2,1)S(1)}, u32[]{:S(2)}, u32[]{:S(2)}) collective-permute-start(bf16[32,2,4096]{2,1,0:T(2,128)(2,1)S(1)} %collective-permute-done.1), channel_id=1, source_target_pairs={{0,1},{1,2},{2,3},{3,4},{4,5},{5,6},{6,7},{7,8},{8,9},{9,10},{10,1... | collective-permute-start | bytes 1572872 | tf_op jit(solution)/shard_map/ppermute | solution.py:20
  182.5 17.3 %collective-permute-start.4 = (bf16[32,2,4096]{2,1,0:T(2,128)(2,1)S(1)}, bf16[32,2,4096]{2,1,0:T(2,128)(2,1)S(1)}, u32[]{:S(2)}, u32[]{:S(2)}) collective-permute-start(bf16[32,2,4096]{2,1,0:T(2,128)(2,1)S(1)} %collective-permute-done.2), channel_id=1, source_target_pairs={{0,15},{1,0},{2,1},{3,2},{4,3},{5,4},{6,5},{7,6},{8,7},{9,8},{10,9... | collective-permute-start | bytes 1572872 | tf_op jit(solution)/shard_map/ppermute | solution.py:25
  197.9 16.5 %collective-permute-start.5 = (bf16[32,2,4096]{2,1,0:T(2,128)(2,1)S(1)}, bf16[32,2,4096]{2,1,0:T(2,128)(2,1)S(1)}, u32[]{:S(2)}, u32[]{:S(2)}) collective-permute-start(bf16[32,2,4096]{2,1,0:T(2,128)(2,1)S(1)} %collective-permute-done.3), channel_id=1, source_target_pairs={{0,1},{1,2},{2,3},{3,4},{4,5},{5,6},{6,7},{7,8},{8,9},{9,10},{10,1... | collective-permute-start | bytes 1572872 | tf_op jit(solution)/shard_map/ppermute | solution.py:20
  199.8 16.5 %collective-permute-start.6 = (bf16[32,2,4096]{2,1,0:T(2,128)(2,1)S(1)}, bf16[32,2,4096]{2,1,0:T(2,128)(2,1)S(1)}, u32[]{:S(2)}, u32[]{:S(2)}) collective-permute-start(bf16[32,2,4096]{2,1,0:T(2,128)(2,1)S(1)} %collective-permute-done.4), channel_id=1, source_target_pairs={{0,15},{1,0},{2,1},{3,2},{4,3},{5,4},{6,5},{7,6},{8,7},{9,8},{10,9... | collective-permute-start | bytes 1572872 | tf_op jit(solution)/shard_map/ppermute | solution.py:25
  214.3 15.6 %collective-permute-start.7 = (bf16[32,2,4096]{2,1,0:T(2,128)(2,1)S(1)}, bf16[32,2,4096]{2,1,0:T(2,128)(2,1)S(1)}, u32[]{:S(2)}, u32[]{:S(2)}) collective-permute-start(bf16[32,2,4096]{2,1,0:T(2,128)(2,1)S(1)} %collective-permute-done.5), channel_id=1, source_target_pairs={{0,1},{1,2},{2,3},{3,4},{4,5},{5,6},{6,7},{7,8},{8,9},{9,10},{10,1... | collective-permute-start | bytes 1572872 | tf_op jit(solution)/shard_map/ppermute | solution.py:20
  216.3 15.6 %collective-permute-start.8 = (bf16[32,2,4096]{2,1,0:T(2,128)(2,1)S(1)}, bf16[32,2,4096]{2,1,0:T(2,128)(2,1)S(1)}, u32[]{:S(2)}, u32[]{:S(2)}) collective-permute-start(bf16[32,2,4096]{2,1,0:T(2,128)(2,1)S(1)} %collective-permute-done.6), channel_id=1, source_target_pairs={{0,15},{1,0},{2,1},{3,2},{4,3},{5,4},{6,5},{7,6},{8,7},{9,8},{10,9... | collective-permute-start | bytes 1572872 | tf_op jit(solution)/shard_map/ppermute | solution.py:25
  229.9 14.8 %collective-permute-start.9 = (bf16[32,2,4096]{2,1,0:T(2,128)(2,1)S(1)}, bf16[32,2,4096]{2,1,0:T(2,128)(2,1)S(1)}, u32[]{:S(2)}, u32[]{:S(2)}) collective-permute-start(bf16[32,2,4096]{2,1,0:T(2,128)(2,1)S(1)} %collective-permute-done.7), channel_id=1, source_target_pairs={{0,1},{1,2},{2,3},{3,4},{4,5},{5,6},{6,7},{7,8},{8,9},{9,10},{10,1... | collective-permute-start | bytes 1572872 | tf_op jit(solution)/shard_map/ppermute | solution.py:20
  231.9 14.8 %collective-permute-start.10 = (bf16[32,2,4096]{2,1,0:T(2,128)(2,1)S(1)}, bf16[32,2,4096]{2,1,0:T(2,128)(2,1)S(1)}, u32[]{:S(2)}, u32[]{:S(2)}) collective-permute-start(bf16[32,2,4096]{2,1,0:T(2,128)(2,1)S(1)} %collective-permute-done.8), channel_id=1, source_target_pairs={{0,15},{1,0},{2,1},{3,2},{4,3},{5,4},{6,5},{7,6},{8,7},{9,8},{10,9... | collective-permute-start | bytes 1572872 | tf_op jit(solution)/shard_map/ppermute | solution.py:25
  244.7 13.9 %collective-permute-start.11 = (bf16[32,2,4096]{2,1,0:T(2,128)(2,1)S(1)}, bf16[32,2,4096]{2,1,0:T(2,128)(2,1)S(1)}, u32[]{:S(2)}, u32[]{:S(2)}) collective-permute-start(bf16[32,2,4096]{2,1,0:T(2,128)(2,1)S(1)} %collective-permute-done.9), channel_id=1, source_target_pairs={{0,1},{1,2},{2,3},{3,4},{4,5},{5,6},{6,7},{7,8},{8,9},{9,10},{10,1... | collective-permute-start | bytes 1572872 | tf_op jit(solution)/shard_map/ppermute | solution.py:20
  246.6 13.9 %collective-permute-start.12 = (bf16[32,2,4096]{2,1,0:T(2,128)(2,1)S(1)}, bf16[32,2,4096]{2,1,0:T(2,128)(2,1)S(1)}, u32[]{:S(2)}, u32[]{:S(2)}) collective-permute-start(bf16[32,2,4096]{2,1,0:T(2,128)(2,1)S(1)} %collective-permute-done.10), channel_id=1, source_target_pairs={{0,15},{1,0},{2,1},{3,2},{4,3},{5,4},{6,5},{7,6},{8,7},{9,8},{10,9... | collective-permute-start | bytes 1572872 | tf_op jit(solution)/shard_map/ppermute | solution.py:25
  254.1 34.4 %copy-start.8 = (bf16[1,4096,64]{1,2,0:T(8,128)(2,1)S(1)}, bf16[1,4096,64]{1,2,0:T(8,128)(2,1)}, u32[]{:S(2)}) copy-start(bf16[1,4096,64]{1,2,0:T(8,128)(2,1)} %param.29) | copy-start | bytes 1572868
  258.6 13.2 %collective-permute-start.13 = (bf16[32,2,4096]{2,1,0:T(2,128)(2,1)S(1)}, bf16[32,2,4096]{2,1,0:T(2,128)(2,1)S(1)}, u32[]{:S(2)}, u32[]{:S(2)}) collective-permute-start(bf16[32,2,4096]{2,1,0:T(2,128)(2,1)S(1)} %collective-permute-done.11), channel_id=1, source_target_pairs={{0,1},{1,2},{2,3},{3,4},{4,5},{5,6},{6,7},{7,8},{8,9},{9,10},{10,1... | collective-permute-start | bytes 1572872 | tf_op jit(solution)/shard_map/ppermute | solution.py:20
  260.5 14.2 %collective-permute-start.14 = (bf16[32,2,4096]{2,1,0:T(2,128)(2,1)S(1)}, bf16[32,2,4096]{2,1,0:T(2,128)(2,1)S(1)}, u32[]{:S(2)}, u32[]{:S(2)}) collective-permute-start(bf16[32,2,4096]{2,1,0:T(2,128)(2,1)S(1)} %collective-permute-done.12), channel_id=1, source_target_pairs={{0,15},{1,0},{2,1},{3,2},{4,3},{5,4},{6,5},{7,6},{8,7},{9,8},{10,9... | collective-permute-start | bytes 1572872 | tf_op jit(solution)/shard_map/ppermute | solution.py:25
  271.8 13.2 %collective-permute-start.15 = (bf16[32,2,4096]{2,1,0:T(2,128)(2,1)S(1)}, bf16[32,2,4096]{2,1,0:T(2,128)(2,1)S(1)}, u32[]{:S(2)}, u32[]{:S(2)}) collective-permute-start(bf16[32,2,4096]{2,1,0:T(2,128)(2,1)S(1)} %collective-permute-done.13), channel_id=1, source_target_pairs={{0,1},{1,2},{2,3},{3,4},{4,5},{5,6},{6,7},{7,8},{8,9},{9,10},{10,1... | collective-permute-start | bytes 1572872 | tf_op jit(solution)/shard_map/ppermute | solution.py:20
  285.9 65.4 %copy-start.9 = (bf16[1,1024,256]{2,1,0:T(8,128)(2,1)S(1)}, bf16[1,1024,256]{2,1,0:T(8,128)(2,1)}, u32[]{:S(2)}) copy-start(bf16[1,1024,256]{2,1,0:T(8,128)(2,1)} %param.30) | copy-start | bytes 1572868
  291.2 78.2 %copy-start.6 = (f32[256,2]{0,1:T(2,128)S(1)}, f32[256,2]{0,1:T(2,128)}, u32[]{:S(2)}) copy-start(f32[256,2]{0,1:T(2,128)} %param.27) | copy-start | bytes 6148
  291.3 114.7 %copy-start.3 = (bf16[1024,256]{1,0:T(8,128)(2,1)S(1)}, bf16[1024,256]{1,0:T(8,128)(2,1)}, u32[]{:S(2)}) copy-start(bf16[1024,256]{1,0:T(8,128)(2,1)} %param.33) | copy-start | bytes 1572868
  354.4 47.8 %all-to-all-start.5 = ((bf16[32,32,256]{2,1,0:T(8,128)(2,1)}), bf16[32,32,256]{2,1,0:T(8,128)(2,1)S(1)}, u32[]{:S(2)}, u32[]{:S(2)}) async-start(bf16[32,32,256]{2,1,0:T(8,128)(2,1)} %bitcast.44), calls=%async_computation.5 | async-start | bytes 1048576 | tf_op jit(solution)/shard_map/all_to_all | solution.py:171
Sparse Core Ops, SparseCore 0:
  292.1 59.1 all-gather.1
